TPU v7x, 32 devices: a whole 2x2x4 slice. The times are simulated.
32 devices in a mesh: ra: 4 (over y, x), cb: 8 (over z, core).
Axes of the slice: x: 2, y: 2, z: 4, core: 2. Of those that a mesh axis runs over, the one named last changes fastest.
Arguments:
- tokens: bfloat16 [512, 4096], P(None, 'ra'), may hold values from -40 to 40, as said below
- norm_gain: float32 [2, 4096], P(None, 'ra'), may hold values from 0.1 to 1.9
- gate_weight: bfloat16 [2, 4096, 11264], P(None, 'ra', 'cb'), may hold values from -0.09375 to 0.09375
- up_weight: bfloat16 [2, 4096, 11264], P(None, 'ra', 'cb'), may hold values from -0.09375 to 0.09375
- down_weight: bfloat16 [2, 11264, 4096], P(None, 'cb', 'ra'), may hold values from -0.0546875 to 0.0546875
Outputs:
- result: bfloat16 [512, 4096], P(None, 'ra')
Inputs may be any that keep to these rules, and one draw needn't show every extreme that they name: `tokens`: features come in blocks of 32 with scales that differ from block to block by up to a factor of 16.
All inputs are finite; a program needn't handle non-finite values.
Results may differ from a plain program's by a relative error of at most 0.0075.
Values may be sent and summed in bfloat16 or wider, within the bound.
A program may use at most 64 MiB of HBM per device.

v0:
```python
import jax
import jax.numpy as jnp
from jax import lax
from jax.sharding import PartitionSpec as P

D = 4096
LAYERS = 2
epsilon = 1e-06
keep_share = 0.5


def body(tokens, norm_gain, gate_weight, up_weight, down_weight):
    stream = tokens
    for layer in range(LAYERS):
        widened = stream.astype(jnp.float32)
        squares = jnp.sum(widened * widened, axis=1)
        normed = (widened * norm_gain[layer]).astype(jnp.bfloat16)
        gate_part = jnp.dot(normed, gate_weight[layer], preferred_element_type=jnp.float32)
        up_part = jnp.dot(normed, up_weight[layer], preferred_element_type=jnp.float32)
        total = lax.psum(squares, "ra")
        gate_share, up_share = (
            lax.psum_scatter(gate_part, "ra", scatter_dimension=1, tiled=True),
            lax.psum_scatter(up_part, "ra", scatter_dimension=1, tiled=True),
        )
        scale = lax.rsqrt(total / D + epsilon)[:, None]
        share = (jax.nn.silu(gate_share * scale) * (up_share * scale)).astype(jnp.bfloat16)
        hidden = lax.all_gather(share, "ra", axis=1, tiled=True)
        partial_down = jnp.dot(hidden, down_weight[layer], preferred_element_type=jnp.float32)
        branch = lax.psum(partial_down, "cb")
        stream = (keep_share * widened + branch).astype(jnp.bfloat16)
    return stream


def solution(mesh):
    placed = (
        P(None, "ra"),
        P(None, "ra"),
        P(None, "ra", "cb"),
        P(None, "ra", "cb"),
        P(None, "cb", "ra"),
    )
    return jax.shard_map(body, mesh=mesh, in_specs=placed, out_specs=P(None, "ra"), check_vma=False)
```

profile of v0, /device:TPU:0, one launch (start us, length us, event | category | flops | bytes accessed | tf_op | source)
XLA Modules:
  0.0 411.4 jit_solution(7383496427016766130)
XLA Ops:
  6.5 0.0 reduce-scatter.7.cloned.1.call-start
  6.5 0.8 fusion.31
  7.3 5.4 %fusion.8 = f32[512,1408]{0,1:T(8,128)} fusion(bf16[2,1024,1408]{2,1,0:T(8,128)(2,1)} %param.8, bf16[512,1024]{1,0:T(8,128)(2,1)} %param.5, f32[1024]{0:T(1024)S(1)} %bitcast.24), kind=kOutput, calls=%fused_computation.14 | convolution fusion | flops 1477967872 | bytes 6819840 | tf_op jit(solution)/shard_map/dot_general | solution.py:19
  12.7 0.0 copy-start
  12.7 0.0 reduce-scatter.7.cloned.1.call-update
  12.8 0.0 reduce-scatter.5.cloned.1.call-start
  12.8 1.1 copy-done
  14.0 5.1 %fusion.10 = f32[512,1408]{0,1:T(8,128)} fusion(bf16[2,1024,1408]{2,1,0:T(8,128)(2,1)} %param.7, bf16[512,1024]{1,0:T(8,128)(2,1)S(1)} %copy-done, f32[1024]{0:T(1024)S(1)} %bitcast.25), kind=kOutput, calls=%fused_computation.16 | convolution fusion | flops 1477967872 | bytes 6819840 | tf_op jit(solution)/shard_map/dot_general | solution.py:18
  19.1 0.0 reduce-scatter.5.cloned.1.call-update
  19.1 0.0 all-gather.3.cloned.1.call-start
  19.2 0.3 fusion.21
  19.5 11.9 %psum.28 = f32[512]{0:T(512)S(1)} all-reduce(f32[512]{0:T(512)S(1)} %fusion.21), channel_id=1, replica_groups=mesh['ra'=4,'cb'=8] {'ra'}, use_global_device_ids=true, to_apply=%region_2.0 | all-reduce | flops 512 | bytes 4096 | tf_op jit(solution)/shard_map/psum | solution.py:20
  31.4 26.3 %reduce-scatter.7.cloned.1.call-done = f32[512,352]{0,1:T(8,128)} async-done(((f32[512,1408]{0,1:T(8,128)}), f32[512,352]{0,1:T(8,128)}) %reduce-scatter.7.cloned.1.call-update) | async-done | bytes 720912 | tf_op jit(solution)/shard_map/reduce_scatter | solution.py:23
  57.6 44.8 %reduce-scatter.5.cloned.1.call-done = f32[512,352]{0,1:T(8,128)} async-done(((f32[512,1408]{0,1:T(8,128)}), f32[512,352]{0,1:T(8,128)}) %reduce-scatter.5.cloned.1.call-update) | async-done | bytes 720912 | tf_op jit(solution)/shard_map/reduce_scatter | solution.py:22
  102.4 2.3 multiply_convert_fusion.1
  104.7 0.0 all-gather.3.cloned.1.call-update
  104.7 0.0 all-reduce.3.cloned.1.call-start
  104.8 29.8 %all-gather.3.cloned.1.call-done = bf16[512,1408]{0,1:T(8,128)(2,1)} async-done(((bf16[512,352]{0,1:T(8,128)(2,1)}), bf16[512,1408]{0,1:T(8,128)(2,1)}) %all-gather.3.cloned.1.call-update) | async-done | bytes 1441808 | tf_op jit(solution)/shard_map/all_gather | solution.py:27
  134.6 5.4 %fusion.6 = f32[512,1024]{1,0:T(8,128)} fusion(bf16[512,1408]{0,1:T(8,128)(2,1)} %all-gather.3.cloned.1.call-done, bf16[2,1408,1024]{2,1,0:T(8,128)(2,1)} %param.9), kind=kOutput, calls=%fused_computation.12 | convolution fusion | flops 1476395008 | bytes 6422528 | tf_op jit(solution)/shard_map/dot_general | solution.py:28
  140.1 0.0 all-reduce.3.cloned.1.call-update
  140.1 0.0 reduce-scatter.9.cloned.1.call-start
  140.1 65.2 %all-reduce.3.cloned.1.call-done = f32[512,1024]{1,0:T(8,128)} async-done(((f32[512,1024]{1,0:T(8,128)}), f32[512,1024]{1,0:T(8,128)}) %all-reduce.3.cloned.1.call-update) | async-done | bytes 2097168 | tf_op jit(solution)/shard_map/psum | solution.py:29
  205.3 2.0 fusion.25
  207.4 5.1 %fusion.4 = f32[512,1408]{0,1:T(8,128)} fusion(bf16[2,1024,1408]{2,1,0:T(8,128)(2,1)} %param.7, bf16[512,1024]{1,0:T(8,128)(2,1)S(1)} %get-tuple-element.6, f32[1024]{0:T(1024)S(1)} %bitcast.22), kind=kOutput, calls=%fused_computation.10 | convolution fusion | flops 1477967872 | bytes 6819840 | tf_op jit(solution)/shard_map/dot_general | solution.py:18
  212.4 0.0 reduce-scatter.9.cloned.1.call-update
  212.5 0.0 reduce-scatter.11.cloned.1.call-start
  212.5 5.1 %fusion.2 = f32[512,1408]{0,1:T(8,128)} fusion(bf16[2,1024,1408]{2,1,0:T(8,128)(2,1)} %param.8, bf16[512,1024]{1,0:T(8,128)(2,1)S(1)} %get-tuple-element.6, f32[1024]{0:T(1024)S(1)} %bitcast.23), kind=kOutput, calls=%fused_computation.8 | convolution fusion | flops 1477967872 | bytes 6819840 | tf_op jit(solution)/shard_map/dot_general | solution.py:19
  217.7 0.0 reduce-scatter.11.cloned.1.call-update
  217.7 0.0 all-gather.5.cloned.1.call-start
  217.7 10.4 %psum.30 = f32[512]{0:T(512)S(1)} all-reduce(f32[512]{0:T(512)S(1)} %get-tuple-element.5), channel_id=1, replica_groups=mesh['ra'=4,'cb'=8] {'ra'}, use_global_device_ids=true, to_apply=%region_7.8 | all-reduce | flops 512 | bytes 4096 | tf_op jit(solution)/shard_map/psum | solution.py:20
  228.1 26.0 %reduce-scatter.9.cloned.1.call-done = f32[512,352]{0,1:T(8,128)} async-done(((f32[512,1408]{0,1:T(8,128)}), f32[512,352]{0,1:T(8,128)}) %reduce-scatter.9.cloned.1.call-update) | async-done | bytes 720912 | tf_op jit(solution)/shard_map/reduce_scatter | solution.py:22
  254.1 44.7 %reduce-scatter.11.cloned.1.call-done = f32[512,352]{0,1:T(8,128)} async-done(((f32[512,1408]{0,1:T(8,128)}), f32[512,352]{0,1:T(8,128)}) %reduce-scatter.11.cloned.1.call-update) | async-done | bytes 720912 | tf_op jit(solution)/shard_map/reduce_scatter | solution.py:23
  298.8 2.3 multiply_convert_fusion
  301.1 0.0 all-gather.5.cloned.1.call-update
  301.1 0.0 all-reduce.5.cloned.1.call-start
  301.1 29.9 %all-gather.5.cloned.1.call-done = bf16[512,1408]{0,1:T(8,128)(2,1)} async-done(((bf16[512,352]{0,1:T(8,128)(2,1)}), bf16[512,1408]{0,1:T(8,128)(2,1)}) %all-gather.5.cloned.1.call-update) | async-done | bytes 1441808 | tf_op jit(solution)/shard_map/all_gather | solution.py:27
  331.0 5.4 %fusion = f32[512,1024]{1,0:T(8,128)} fusion(bf16[512,1408]{0,1:T(8,128)(2,1)} %all-gather.5.cloned.1.call-done, bf16[2,1408,1024]{2,1,0:T(8,128)(2,1)} %param.9), kind=kOutput, calls=%fused_computation.6 | convolution fusion | flops 1476395008 | bytes 6422528 | tf_op jit(solution)/shard_map/dot_general | solution.py:28
  336.4 0.0 all-reduce.5.cloned.1.call-update
  336.5 65.2 %all-reduce.5.cloned.1.call-done = f32[512,1024]{1,0:T(8,128)} async-done(((f32[512,1024]{1,0:T(8,128)}), f32[512,1024]{1,0:T(8,128)}) %all-reduce.5.cloned.1.call-update) | async-done | bytes 2097168 | tf_op jit(solution)/shard_map/psum | solution.py:29
  401.7 2.9 fusion.23
  (2 shorter events, 0.0 us)
Async XLA Ops:
  6.5 51.1 %reduce-scatter.7.cloned.1.call-start = ((), (), s32[]{:S(2)}) async-start(), calls=%async_computation.5 | async-start | bytes 3604480 | tf_op jit(solution)/shard_map/reduce_scatter | solution.py:23
  12.7 1.2 copy-start
  12.8 89.7 %reduce-scatter.5.cloned.1.call-start = ((), (), s32[]{:S(2)}) async-start(), calls=%async_computation.4 | async-start | bytes 3604480 | tf_op jit(solution)/shard_map/reduce_scatter | solution.py:22
  19.1 115.5 %all-gather.3.cloned.1.call-start = ((), (), s32[]{:S(2)}) async-start(), calls=%async_computation.6 | async-start | bytes 1802240 | tf_op jit(solution)/shard_map/all_gather | solution.py:27
  104.7 100.6 %all-reduce.3.cloned.1.call-start = ((), (), s32[]{:S(2)}) async-start(), calls=%async_computation.7 | async-start | bytes 4194304 | tf_op jit(solution)/shard_map/psum | solution.py:29
  140.1 114.1 %reduce-scatter.9.cloned.1.call-start = ((), (), s32[]{:S(2)}) async-start(), calls=%async_computation.8 | async-start | bytes 3604480 | tf_op jit(solution)/shard_map/reduce_scatter | solution.py:22
  212.5 86.3 %reduce-scatter.11.cloned.1.call-start = ((), (), s32[]{:S(2)}) async-start(), calls=%async_computation.9 | async-start | bytes 3604480 | tf_op jit(solution)/shard_map/reduce_scatter | solution.py:23
  217.7 113.3 %all-gather.5.cloned.1.call-start = ((), (), s32[]{:S(2)}) async-start(), calls=%async_computation.10 | async-start | bytes 1802240 | tf_op jit(solution)/shard_map/all_gather | solution.py:27
  301.1 100.6 %all-reduce.5.cloned.1.call-start = ((), (), s32[]{:S(2)}) async-start(), calls=%async_computation.11 | async-start | bytes 4194304 | tf_op jit(solution)/shard_map/psum | solution.py:29
Sparse Core Ops, SparseCore 0:
  12.9 44.7 reduce-scatter.6
  60.7 41.7 reduce-scatter.4
  104.9 29.7 all-gather.2
  140.2 65.0 all-reduce.2
  212.6 41.4 reduce-scatter.8
  257.0 41.7 reduce-scatter.10
  301.2 29.7 all-gather.4
  336.6 65.0 all-reduce.4
where the time goes:
time: 412 us; the launch traced here: 411 us
  waiting for transfers between devices  332 us (81%)
  matrix products  31.6 us (8%)
  blocking collectives  22.2 us (5%)
  between operations  13.5 us (3%)
  other arithmetic  9.81 us (2%)
    psum x2, waiting for transfers between devices, body(): branch = lax.psum(partial_down, 'cb')  130 us
    reduce_scatter x2, waiting for transfers between devices, body(): lax.psum_scatter(up_part, 'ra', scatter_dimension=1, tiled=True)  70.9 us
    reduce_scatter x2, waiting for transfers between devices, body(): lax.psum_scatter(gate_part, 'ra', scatter_dimension=1, tiled=True)  70.8 us
    all_gather x2, waiting for transfers between devices, body(): hidden = lax.all_gather(share, 'ra', axis=1, tiled=True)  59.7 us
    psum x2, blocking collectives, body(): total = lax.psum(squares, 'ra')  22.2 us
    dot_general x2, matrix products, body(): jnp.dot(hidden, down_weight[layer], preferred_element_type=jnp.float32)  10.8 us
    dot_general x2, matrix products, body(): jnp.dot(normed, up_weight[layer], preferred_element_type=jnp.float32)  10.6 us
    dot_general x2, matrix products, body(): jnp.dot(normed, gate_weight[layer], preferred_element_type=jnp.float32)  10.2 us
  transfers between devices with their start and end apart: 8, of which 8 were waited for; matrix products, arithmetic and copies ran while one was open for 3% of the time, Pallas kernels for 0%

commit v1 on v0

--- a/solution.py
+++ b/solution.py
@@ -7,6 +7,15 @@
 LAYERS = 2
 epsilon = 1e-06
 keep_share = 0.5
+
+
+def add_in_pairs(x, axis):
+    count = lax.axis_size(axis)
+    total, far = (x, 1)
+    while far < count:
+        total = total + lax.ppermute(total, axis, [(i, i ^ far) for i in range(count)])
+        far = 2 * far
+    return total
 
 
 def body(tokens, norm_gain, gate_weight, up_weight, down_weight):
@@ -26,7 +35,7 @@
         share = (jax.nn.silu(gate_share * scale) * (up_share * scale)).astype(jnp.bfloat16)
         hidden = lax.all_gather(share, "ra", axis=1, tiled=True)
         partial_down = jnp.dot(hidden, down_weight[layer], preferred_element_type=jnp.float32)
-        branch = lax.psum(partial_down, "cb")
+        branch = add_in_pairs(partial_down, "cb")
         stream = (keep_share * widened + branch).astype(jnp.bfloat16)
     return stream
 

time: 412 us -> 566 us (1.37)
  waiting for transfers between devices: 332 us -> 484 us
  starting transfers between devices: 0.3 us -> 8.4 us
    ppermute x0 -> x6, waiting for transfers between devices: none -> 281 us  [add_in_pairs(): lax.ppermute(total, axis, [(i, i ^ far) for i in range(count)])]
    psum x2 -> x0, waiting for transfers between devices: 130 us -> none  [body(): branch = lax.psum(partial_down, 'cb')]
    ppermute x0 -> x6, starting transfers between devices: none -> 8.19 us  [add_in_pairs(): lax.ppermute(total, axis, [(i, i ^ far) for i in range(count)])]
  transfers between devices with their start and end apart: 8 -> 12, of which waited for: 8 -> 12; matrix products, arithmetic and copies ran while one was open for 3% -> 2% of each run, Pallas kernels for 0% -> 0%
where the time goes in v1:
time: 566 us; the launch traced here: 565 us
  waiting for transfers between devices  484 us (86%)
  matrix products  27.1 us (5%)
  blocking collectives  21.5 us (4%)
  between operations  13.6 us (2%)
  other arithmetic  8.98 us (2%)
  starting transfers between devices  8.4 us (1%)
    ppermute x6, waiting for transfers between devices, add_in_pairs(): lax.ppermute(total, axis, [(i, i ^ far) for i in range(count)])  281 us
    reduce_scatter x2, waiting for transfers between devices, body(): lax.psum_scatter(gate_part, 'ra', scatter_dimension=1, tiled=True)  72 us
    reduce_scatter x2, waiting for transfers between devices, body(): lax.psum_scatter(up_part, 'ra', scatter_dimension=1, tiled=True)  70.9 us
    all_gather x2, waiting for transfers between devices, body(): hidden = lax.all_gather(share, 'ra', axis=1, tiled=True)  59.7 us
    psum x2, blocking collectives, body(): total = lax.psum(squares, 'ra')  21.5 us
  transfers between devices with their start and end apart: 12, of which 12 were waited for; matrix products, arithmetic and copies ran while one was open for 2% of the time, Pallas kernels for 0%

profile of v1, /device:TPU:0, one launch (start us, length us, event | category | flops | bytes accessed | tf_op | source)
XLA Modules:
  0.0 565.5 jit_solution(5909414072514984765)
XLA Ops:
  6.5 0.8 fusion.31
  7.3 5.4 fusion.8
  12.7 0.0 reduce-scatter.7.cloned.1.call-update
  12.8 0.0 reduce-scatter.5.cloned.1.call-start
  12.8 1.1 copy-done
  14.0 5.1 fusion.10
  19.1 0.0 reduce-scatter.5.cloned.1.call-update
  19.1 0.0 all-gather.3.cloned.1.call-start
  19.2 0.3 fusion.21
  19.4 11.9 %psum.14 = f32[512]{0:T(512)S(1)} all-reduce(f32[512]{0:T(512)S(1)} %fusion.21), channel_id=1, replica_groups=mesh['ra'=4,'cb'=8] {'ra'}, use_global_device_ids=true, to_apply=%region_2.0 | all-reduce | flops 512 | bytes 4096 | tf_op jit(solution)/shard_map/psum | solution.py:29
  31.3 26.3 %reduce-scatter.7.cloned.1.call-done = f32[512,352]{0,1:T(8,128)} async-done(((f32[512,1408]{0,1:T(8,128)}), f32[512,352]{0,1:T(8,128)}) %reduce-scatter.7.cloned.1.call-update) | async-done | bytes 720912 | tf_op jit(solution)/shard_map/reduce_scatter | solution.py:32
  57.6 44.8 %reduce-scatter.5.cloned.1.call-done = f32[512,352]{0,1:T(8,128)} async-done(((f32[512,1408]{0,1:T(8,128)}), f32[512,352]{0,1:T(8,128)}) %reduce-scatter.5.cloned.1.call-update) | async-done | bytes 720912 | tf_op jit(solution)/shard_map/reduce_scatter | solution.py:31
  102.4 2.3 multiply_convert_fusion.1
  104.7 0.0 all-gather.3.cloned.1.call-update
  104.7 0.0 reduce-scatter.9.cloned.1.call-start
  104.8 29.8 %all-gather.3.cloned.1.call-done = bf16[512,1408]{0,1:T(8,128)(2,1)} async-done(((bf16[512,352]{0,1:T(8,128)(2,1)}), bf16[512,1408]{0,1:T(8,128)(2,1)}) %all-gather.3.cloned.1.call-update) | async-done | bytes 1441808 | tf_op jit(solution)/shard_map/all_gather | solution.py:36
  134.6 4.1 fusion.6
  138.7 0.1 collective-permute-start
  138.8 4.1 collective-permute-done
  142.9 0.6 add.51
  143.5 1.6 collective-permute-start.1
  145.0 46.2 %collective-permute-done.1 = f32[512,1024]{1,0:T(8,128)S(1)} collective-permute-done((f32[512,1024]{1,0:T(8,128)S(1)}, f32[512,1024]{1,0:T(8,128)S(1)}, u32[]{:S(2)}, u32[]{:S(2)}) %collective-permute-start.1) | collective-permute-done | bytes 2097184 | tf_op jit(solution)/shard_map/ppermute | solution.py:16
  191.2 0.4 add.52
  191.7 2.5 collective-permute-start.2
  194.1 90.2 %collective-permute-done.2 = f32[512,1024]{1,0:T(8,128)S(1)} collective-permute-done((f32[512,1024]{1,0:T(8,128)S(1)}, f32[512,1024]{1,0:T(8,128)S(1)}, u32[]{:S(2)}, u32[]{:S(2)}) %collective-permute-start.2) | collective-permute-done | bytes 2097184 | tf_op jit(solution)/shard_map/ppermute | solution.py:16
  284.4 0.6 fusion.25
  285.0 3.3 fusion.4
  288.3 0.0 reduce-scatter.9.cloned.1.call-update
  288.3 0.0 reduce-scatter.11.cloned.1.call-start
  288.3 5.1 fusion.2
  293.5 0.0 reduce-scatter.11.cloned.1.call-update
  293.5 0.0 all-gather.5.cloned.1.call-start
  293.5 9.6 %psum.15 = f32[512]{0:T(512)S(1)} all-reduce(f32[512]{0:T(512)S(1)} %get-tuple-element.5), channel_id=1, replica_groups=mesh['ra'=4,'cb'=8] {'ra'}, use_global_device_ids=true, to_apply=%region_6.7 | all-reduce | flops 512 | bytes 4096 | tf_op jit(solution)/shard_map/psum | solution.py:29
  303.2 27.2 %reduce-scatter.9.cloned.1.call-done = f32[512,352]{0,1:T(8,128)} async-done(((f32[512,1408]{0,1:T(8,128)}), f32[512,352]{0,1:T(8,128)}) %reduce-scatter.9.cloned.1.call-update) | async-done | bytes 720912 | tf_op jit(solution)/shard_map/reduce_scatter | solution.py:31
  330.4 44.7 %reduce-scatter.11.cloned.1.call-done = f32[512,352]{0,1:T(8,128)} async-done(((f32[512,1408]{0,1:T(8,128)}), f32[512,352]{0,1:T(8,128)}) %reduce-scatter.11.cloned.1.call-update) | async-done | bytes 720912 | tf_op jit(solution)/shard_map/reduce_scatter | solution.py:32
  375.0 2.3 multiply_convert_fusion
  377.3 0.0 all-gather.5.cloned.1.call-update
  377.3 29.9 %all-gather.5.cloned.1.call-done = bf16[512,1408]{0,1:T(8,128)(2,1)} async-done(((bf16[512,352]{0,1:T(8,128)(2,1)}), bf16[512,1408]{0,1:T(8,128)(2,1)}) %all-gather.5.cloned.1.call-update) | async-done | bytes 1441808 | tf_op jit(solution)/shard_map/all_gather | solution.py:36
  407.2 4.1 fusion
  411.3 0.1 collective-permute-start.3
  411.4 4.1 collective-permute-done.3
  415.5 0.6 add.57
  416.1 1.6 collective-permute-start.4
  417.6 46.2 %collective-permute-done.4 = f32[512,1024]{1,0:T(8,128)S(1)} collective-permute-done((f32[512,1024]{1,0:T(8,128)S(1)}, f32[512,1024]{1,0:T(8,128)S(1)}, u32[]{:S(2)}, u32[]{:S(2)}) %collective-permute-start.4) | collective-permute-done | bytes 2097184 | tf_op jit(solution)/shard_map/ppermute | solution.py:16
  463.8 0.4 add.58
  464.3 2.5 collective-permute-start.5
  466.7 90.2 %collective-permute-done.5 = f32[512,1024]{1,0:T(8,128)S(1)} collective-permute-done((f32[512,1024]{1,0:T(8,128)S(1)}, f32[512,1024]{1,0:T(8,128)S(1)}, u32[]{:S(2)}, u32[]{:S(2)}) %collective-permute-start.5) | collective-permute-done | bytes 2097184 | tf_op jit(solution)/shard_map/ppermute | solution.py:16
  557.0 1.6 fusion.23
  (9 shorter events, 0.0 us)
Async XLA Ops:
  6.5 51.1 %reduce-scatter.7.cloned.1.call-start = ((), (), s32[]{:S(2)}) async-start(), calls=%async_computation.5 | async-start | bytes 3604480 | tf_op jit(solution)/shard_map/reduce_scatter | solution.py:32
  12.7 1.2 copy-start
  12.8 89.7 %reduce-scatter.5.cloned.1.call-start = ((), (), s32[]{:S(2)}) async-start(), calls=%async_computation.4 | async-start | bytes 3604480 | tf_op jit(solution)/shard_map/reduce_scatter | solution.py:31
  19.1 115.5 %all-gather.3.cloned.1.call-start = ((), (), s32[]{:S(2)}) async-start(), calls=%async_computation.6 | async-start | bytes 1802240 | tf_op jit(solution)/shard_map/all_gather | solution.py:36
  104.7 225.6 %reduce-scatter.9.cloned.1.call-start = ((), (), s32[]{:S(2)}) async-start(), calls=%async_computation.7 | async-start | bytes 3604480 | tf_op jit(solution)/shard_map/reduce_scatter | solution.py:31
  138.7 4.2 collective-permute-start
  142.9 142.0 %slice-start = ((s8[5767168]{0:T(1024)(128)(4,1)}), s8[4194304]{0:T(1024)(128)(4,1)S(1)}, s32[]{:S(2)}) async-start(s8[5767168]{0:T(1024)(128)(4,1)} %bitcast.26), calls=%async_computation.10 | async-start | bytes 8388608
  143.5 141.5 %slice-start.1 = ((s8[5767168]{0:T(1024)(128)(4,1)}), s8[1572864]{0:T(1024)(128)(4,1)S(1)}, s32[]{:S(2)}) async-start(s8[5767168]{0:T(1024)(128)(4,1)} %bitcast.26), calls=%async_computation.11 | async-start | bytes 3145728
  143.5 47.7 %collective-permute-start.1 = (f32[512,1024]{1,0:T(8,128)S(1)}, f32[512,1024]{1,0:T(8,128)S(1)}, u32[]{:S(2)}, u32[]{:S(2)}) collective-permute-start(f32[512,1024]{1,0:T(8,128)S(1)} %add.51), channel_id=1, source_target_pairs={{0,2},{1,3},{2,0},{3,1},{4,6},{5,7},{6,4},{7,5},{8,10},{9,11},{10,... | collective-permute-start | bytes 6291464 | tf_op jit(solution)/shard_map/ppermute | solution.py:16
  191.7 92.7 %collective-permute-start.2 = (f32[512,1024]{1,0:T(8,128)S(1)}, f32[512,1024]{1,0:T(8,128)S(1)}, u32[]{:S(2)}, u32[]{:S(2)}) collective-permute-start(f32[512,1024]{1,0:T(8,128)S(1)} %add.52), channel_id=1, source_target_pairs={{0,4},{1,5},{2,6},{3,7},{4,0},{5,1},{6,2},{7,3},{8,12},{9,13},{10,... | collective-permute-start | bytes 6291464 | tf_op jit(solution)/shard_map/ppermute | solution.py:16
  288.3 86.8 %reduce-scatter.11.cloned.1.call-start = ((), (), s32[]{:S(2)}) async-start(), calls=%async_computation.8 | async-start | bytes 3604480 | tf_op jit(solution)/shard_map/reduce_scatter | solution.py:32
  293.5 113.8 %all-gather.5.cloned.1.call-start = ((), (), s32[]{:S(2)}) async-start(), calls=%async_computation.9 | async-start | bytes 1802240 | tf_op jit(solution)/shard_map/all_gather | solution.py:36
  411.3 4.2 collective-permute-start.3
  416.1 47.7 %collective-permute-start.4 = (f32[512,1024]{1,0:T(8,128)S(1)}, f32[512,1024]{1,0:T(8,128)S(1)}, u32[]{:S(2)}, u32[]{:S(2)}) collective-permute-start(f32[512,1024]{1,0:T(8,128)S(1)} %add.57), channel_id=1, source_target_pairs={{0,2},{1,3},{2,0},{3,1},{4,6},{5,7},{6,4},{7,5},{8,10},{9,11},{10,... | collective-permute-start | bytes 6291464 | tf_op jit(solution)/shard_map/ppermute | solution.py:16
  464.3 92.7 %collective-permute-start.5 = (f32[512,1024]{1,0:T(8,128)S(1)}, f32[512,1024]{1,0:T(8,128)S(1)}, u32[]{:S(2)}, u32[]{:S(2)}) collective-permute-start(f32[512,1024]{1,0:T(8,128)S(1)} %add.58), channel_id=1, source_target_pairs={{0,4},{1,5},{2,6},{3,7},{4,0},{5,1},{6,2},{7,3},{8,12},{9,13},{10,... | collective-permute-start | bytes 6291464 | tf_op jit(solution)/shard_map/ppermute | solution.py:16
Sparse Core Ops, SparseCore 0:
  12.9 44.7 reduce-scatter.6
  60.7 41.7 reduce-scatter.4
  104.9 29.7 all-gather.2
  288.4 41.9 reduce-scatter.8
  333.3 41.7 reduce-scatter.10
  377.5 29.7 all-gather.4
